TPU v7x, 32 devices: a whole 2x2x4 slice. The times are simulated.
32 devices in a mesh: ep: 8 (over z, x), tp: 4 (over y, core).
Axes of the slice: x: 2, y: 2, z: 4, core: 2. Of those that a mesh axis runs over, the one named last changes fastest.
Arguments:
- queries: bfloat16 [4096, 8, 96], P('ep', 'tp'), may hold values from -240 to 240
- kv_latent: bfloat16 [4096, 128], P(('ep', 'tp')), may hold values from -6 to 6
- rope_key: bfloat16 [4096, 32], P(('ep', 'tp')), may hold values from -6 to 6
- kv_gain: float32 [128], replicated, may hold values from 0.1 to 1.9
- kv_up: bfloat16 [128, 8, 128], P(None, 'tp'), may hold values from -0.5 to 0.5
- mix_out: bfloat16 [8, 64, 2048], P('tp'), may hold values from -0.25 to 0.25
- moe_in: bfloat16 [2048, 2048], P('ep', 'tp'), may hold values from -6 to 6
- moe_gain: float32 [2048], replicated, may hold values from 0.1 to 1.9
- routes: int32 [2048, 2], P('ep'), may hold values from 0 to 7, all different within a row; in each aligned block of 256 rows (0 to 255, 256 to 511, ...) at most 68 rows name the same one
- route_weights: float32 [2048, 2], P('ep'), may hold values from 0.1 to 1
- gate_w: bfloat16 [8, 2048, 3584], P('ep', None, 'tp'), may hold values from -0.125 to 0.125
- up_w: bfloat16 [8, 2048, 3584], P('ep', None, 'tp'), may hold values from -0.125 to 0.125
- down_w: bfloat16 [8, 3584, 2048], P('ep', 'tp'), may hold values from -0.09375 to 0.09375
Outputs:
- mixed: bfloat16 [4096, 2048], P(('ep', 'tp'))
- moe_out: bfloat16 [2048, 2048], P('ep', 'tp')
Inputs may be any that keep to these rules, and one draw needn't show every extreme that they name: `routes`: among the rows of one index of ep, no expert is named by more than 68 entries, a bound that some block reaches; a row names 2 different experts.
All inputs are finite; a program needn't handle non-finite values.
Results may differ from a plain program's by a relative error of at most 0.025.
Values may be sent and summed in bfloat16 or wider, within the bound.
A program may use at most 128 MiB of HBM per device.

v0:
```python
import math

import jax
import jax.numpy as jnp
from jax import lax
from jax.sharding import PartitionSpec as P

D = 2048
NOPE = 64
SEQS = 1


eps = 1e-06
rope_base = 10000.0
neg_big = -1e30


def rotate(values, positions):
    half_dim = values.shape[-1] // 2
    inv_freq = rope_base ** (-jnp.arange(half_dim, dtype=jnp.float32) * 2.0 / values.shape[-1])
    angles = positions.astype(jnp.float32)[:, None] * inv_freq[None, :]
    angles = angles.reshape((angles.shape[0],) + (1,) * (values.ndim - 2) + (half_dim,))
    cosine = jnp.cos(angles)
    sine_part = jnp.sin(angles)
    first_half = values[..., :half_dim].astype(jnp.float32)
    second_half = values[..., half_dim:].astype(jnp.float32)
    return jnp.concatenate(
        [
            first_half * cosine - second_half * sine_part,
            second_half * cosine + first_half * sine_part,
        ],
        axis=-1,
    )


def shards(
    queries,
    kv_latent,
    rope_key,
    kv_gain,
    kv_up,
    mix_out,
    moe_in,
    moe_gain,
    routes,
    route_weights,
    gate_w,
    up_w,
    down_w,
):
    block_rows = queries.shape[0]
    heads_here = queries.shape[1]
    value_dim = kv_up.shape[-1] - NOPE
    seq_len = block_rows * lax.axis_size("ep") // SEQS
    query_start = lax.axis_index("ep") * block_rows
    query_index = query_start + jnp.arange(block_rows, dtype=jnp.int32)
    seq_start = query_start // seq_len * seq_len
    query_nope = queries[..., :NOPE]
    query_rot = rotate(queries[..., NOPE:], query_index % seq_len).astype(jnp.bfloat16)
    score_scale = 1.0 / math.sqrt(queries.shape[-1])
    initial = (
        jnp.full((block_rows, heads_here), neg_big, jnp.float32),
        jnp.zeros((block_rows, heads_here), jnp.float32),
        jnp.zeros((block_rows, heads_here, value_dim), jnp.float32),
    )
    latent_piece = lax.all_gather(kv_latent, ("ep", "tp"), axis=0, tiled=True)
    rope_piece = lax.all_gather(rope_key, ("ep", "tp"), axis=0, tiled=True)
    piece_rows = latent_piece.shape[0]
    sub_rows = math.gcd(piece_rows, 512)

    def sub_block(state_in, offset):

        def attend_piece(state_run):
            running_max, running_sum, weighted = state_run
            latent_rows = lax.dynamic_slice_in_dim(latent_piece, offset, sub_rows, 0).astype(
                jnp.float32
            )
            rope_rows = lax.dynamic_slice_in_dim(rope_piece, offset, sub_rows, 0)
            key_ids = offset + jnp.arange(sub_rows, dtype=jnp.int32)
            normed = (
                latent_rows
                * lax.rsqrt(jnp.mean(latent_rows * latent_rows, axis=-1, keepdims=True) + eps)
                * kv_gain
            ).astype(jnp.bfloat16)
            head_proj = jnp.einsum(
                "nr,rhd->nhd", normed, kv_up, preferred_element_type=jnp.float32
            ).astype(jnp.bfloat16)
            key_rot = rotate(rope_rows, key_ids % seq_len).astype(jnp.bfloat16)
            scores = jnp.einsum(
                "qhd,khd->qhk",
                query_nope,
                head_proj[..., :NOPE],
                preferred_element_type=jnp.float32,
            )
            scores = (
                scores
                + jnp.einsum("qhd,kd->qhk", query_rot, key_rot, preferred_element_type=jnp.float32)
            ) * score_scale
            allowed = (
                (key_ids[None, :] <= query_index[:, None]) & (key_ids[None, :] >= seq_start)
            )[:, None, :]
            scores = jnp.where(allowed, scores, neg_big)
            new_max = jnp.maximum(running_max, jnp.max(scores, axis=-1))
            exp_scores = jnp.where(allowed, jnp.exp(scores - new_max[..., None]), 0.0)
            rescale = jnp.exp(running_max - new_max)
            running_sum = running_sum * rescale + jnp.sum(exp_scores, axis=-1)
            weighted = weighted * rescale[..., None] + jnp.einsum(
                "qhk,khd->qhd",
                exp_scores.astype(jnp.bfloat16),
                head_proj[..., NOPE:],
                preferred_element_type=jnp.float32,
            )
            return (new_max, running_sum, weighted)

        is_needed = (offset < query_start + block_rows) & (offset + sub_rows > seq_start)
        return (lax.cond(is_needed, attend_piece, lambda state_run: state_run, state_in), None)

    state_out, _ = lax.scan(
        sub_block, initial, jnp.arange(0, piece_rows, sub_rows, dtype=jnp.int32)
    )
    running_max, running_sum, weighted = state_out
    attn = (weighted / running_sum[..., None]).astype(jnp.bfloat16)
    mixed = lax.psum_scatter(
        jnp.einsum("thv,hvd->td", attn, mix_out, preferred_element_type=jnp.float32).astype(
            jnp.bfloat16
        ),
        "tp",
        scatter_dimension=0,
        tiled=True,
    )
    rows_here = routes.shape[0]
    top_count = routes.shape[1]
    experts = gate_w.shape[0] * lax.axis_size("ep")
    mean_slots = top_count * rows_here // experts
    capacity = mean_slots + max(mean_slots // 16, 1)
    flat_routes = routes.reshape(-1)
    onehot = (flat_routes[:, None] == jnp.arange(experts, dtype=jnp.int32)[None, :]).astype(
        jnp.int32
    )
    slot_rank = jnp.sum((jnp.cumsum(onehot, axis=0) - onehot) * onehot, axis=1)
    slot_dest = flat_routes * capacity + slot_rank
    slot_owner = (
        jnp.full((experts * capacity,), -1, jnp.int32)
        .at[slot_dest]
        .set(jnp.arange(rows_here * top_count, dtype=jnp.int32))
    )
    is_valid = slot_owner >= 0
    token_row = jnp.maximum(slot_owner, 0) // top_count
    send_rows = jnp.where(is_valid[:, None], moe_in[token_row], 0).reshape(
        experts, capacity, moe_in.shape[1]
    )
    arrived = lax.all_to_all(send_rows, "ep", split_axis=0, concat_axis=0, tiled=True)
    piece_f = lax.all_gather(arrived, "tp", axis=2, tiled=True).astype(jnp.float32)
    scaled = (piece_f * moe_gain).astype(jnp.bfloat16)
    gate_rows = gate_w[0]
    up_rows = up_w[0]
    gate_acc = jnp.einsum("scd,df->scf", scaled, gate_rows, preferred_element_type=jnp.float32)
    up_acc = jnp.einsum("scd,df->scf", scaled, up_rows, preferred_element_type=jnp.float32)
    squares = jnp.sum(piece_f * piece_f, axis=-1)
    gate_acc, up_acc, squares = (gate_acc, up_acc, squares)
    row_scale = lax.rsqrt(squares / D + eps)[..., None]
    hidden = (jax.nn.silu(gate_acc * row_scale) * (up_acc * row_scale)).astype(jnp.bfloat16)
    partial_value = jnp.einsum("scf,fd->scd", hidden, down_w[0], preferred_element_type=jnp.float32)
    summed = lax.psum_scatter(
        partial_value.astype(jnp.bfloat16), "tp", scatter_dimension=2, tiled=True
    )
    returned = lax.all_to_all(summed, "ep", split_axis=0, concat_axis=0, tiled=True)
    flat_back = returned.reshape(experts * capacity, returned.shape[-1])
    picked = (
        flat_back[slot_dest].astype(jnp.float32).reshape(rows_here, top_count, returned.shape[-1])
    )
    moe_out = jnp.sum(picked * route_weights[..., None], axis=1).astype(jnp.bfloat16)
    return (mixed, moe_out)


def solution(mesh):
    in_specs = (
        P("ep", "tp", None),
        P(("ep", "tp"), None),
        P(("ep", "tp"), None),
        P(),
        P(None, "tp", None),
        P("tp", None, None),
        P("ep", "tp"),
        P(),
        P("ep", None),
        P("ep", None),
        P("ep", None, "tp"),
        P("ep", None, "tp"),
        P("ep", "tp", None),
    )
    out_specs = (P(("ep", "tp"), None), P("ep", "tp"))
    return jax.shard_map(shards, mesh=mesh, in_specs=in_specs, out_specs=out_specs, check_vma=False)
```

profile of v0, /device:TPU:0, one launch (start us, length us, event | category | flops | bytes accessed | tf_op | source)
XLA Modules:
  0.0 246.8 jit_solution(13989375117769268064)
XLA Ops:
  7.2 0.0 copy-start
  7.2 0.0 all-gather.5.cloned.1.call-start
  7.2 0.9 copy.21
  8.1 0.1 eq.32
  8.3 0.1 eq.28
  8.4 0.7 broadcast_multiply_fusion
  9.1 1.1 reduce-window.6
  10.2 0.2 slice_reduce_fusion
  10.5 0.1 copy.20
  10.6 0.1 mul.192
  10.8 0.1 fusion.67
  10.9 2.4 scatter_custom_fusion
  13.4 2.7 %gather_fusion = bf16[544,512]{1,0:T(8,128)(2,1)S(1)} fusion(bf16[256,512]{1,0:T(8,128)(2,1)S(1)} %copy-done.1, s32[1024]{0:T(1024)S(1)} %pad_clamp_fusion.1), kind=kCustom, calls=%fused_computation | custom fusion | bytes 1116288 | tf_op jit(solution)/shard_map/gather | solution.py:149
  16.1 0.1 gather.9
  16.3 0.1 broadcast_in_dim.71
  16.3 0.1 broadcast_select_fusion
  16.5 0.0 copy-start.8
  16.5 23.7 %all_to_all.10 = bf16[8,68,512]{2,1,0:T(8,128)(2,1)} all-to-all(bf16[8,68,512]{2,1,0:T(8,128)(2,1)S(1)} %broadcast_select_fusion), channel_id=1, replica_groups=mesh['ep'=8,'tp'=4] {'ep'}, dimensions={0} | all-to-all | bytes 1114112 | tf_op jit(solution)/shard_map/all_to_all | solution.py:152
  40.2 0.0 all-gather.5.cloned.1.call-update
  40.2 0.0 all-gather.3.cloned.1.call-start
  40.3 0.7 all-gather.3.cloned.1.call-update
  41.0 0.0 reduce-scatter.5.cloned.1.call-start
  41.0 21.8 %all-gather.5.cloned.1.call-done = bf16[8,68,2048]{2,1,0:T(8,128)(2,1)} async-done(((bf16[8,68,512]{2,1,0:T(8,128)(2,1)}), bf16[8,68,2048]{2,1,0:T(8,128)(2,1)}) %all-gather.5.cloned.1.call-update) | async-done | bytes 2228240 | tf_op jit(solution)/shard_map/all_gather | solution.py:153
  62.9 2.4 fusion.39
  65.3 6.0 %fusion.42 = f32[8,68,896]{2,1,0:T(8,128)} fusion(bf16[1,2048,896]{2,1,0:T(8,128)(2,1)} %param.28, bf16[8,68,2048]{2,1,0:T(8,128)(2,1)S(1)} %copy-done.2, f32[2048]{0:T(1024)S(1)} %copy-done.8), kind=kOutput, calls=%fused_computation.63 | convolution fusion | flops 1999831040 | bytes 7856128 | tf_op jit(solution)/shard_map/scd,df->scf/dot_general | solution.py:158
  71.3 10.5 %fusion.46 = bf16[8,68,2048]{2,1,0:T(8,128)(2,1)} fusion(bf16[1,896,2048]{2,1,0:T(8,128)(2,1)} %param.29, f32[8,68,896]{2,1,0:T(8,128)} %fusion.42, bf16[1,2048,896]{2,1,0:T(8,128)(2,1)} %param.27, bf16[8,68,2048]{2,1,0:T(8,128)(2,1)S(1)} %copy-done.2, f32[2048]{0:T(1024)S(1)} %copy-done.8, f32[8,68]{1,0:T(8,128)S(1)} %add_rsqrt_fusion.1), kind=kOutput, calls=%fused_computation.67 | convolution fusion | flops 4001333248 | bytes 13756544 | tf_op jit(solution)/shard_map/scf,fd->scd/dot_general | solution.py:163
  81.8 0.0 reduce-scatter.5.cloned.1.call-update
  81.8 0.0 reduce-scatter.3.cloned.1.call-start
  81.9 0.8 copy-done.3
  82.7 0.0 copy-done.4
  82.7 0.1 copy.19
  82.9 0.2 multiply_cosine_fusion.1
  83.2 44.1 %all_gather.10 = bf16[4096,32]{0,1:T(8,128)(2,1)} all-gather(bf16[128,32]{0,1:T(8,128)(2,1)S(1)} %copy-done.6), channel_id=1, replica_groups=mesh['ep'=8,'tp'=4] {'ep','tp'}, dimensions={0}, use_global_device_ids=true | all-gather | bytes 270336 | tf_op jit(solution)/shard_map/all_gather | solution.py:67
  127.3 22.8 %while.17 = (s32[]{:T(128)}, f32[512,2]{0,1:T(2,128)S(1)}, f32[512,2]{0,1:T(2,128)S(1)}, f32[512,2,64]{0,2,1:T(8,128)S(1)}, s32[8]{0:T(128)S(1)}, /*index=5*/s32...) while((s32[]{:T(128)}, f32[512,2]{0,1:T(2,128)S(1)}, ...), condition=%wide.region_6.7_spmd.clone, body=%wide.region_0.6_spmd.clone.sunk | while | flops 207981088 | bytes 14346293 | solution.py:118
  127.3 0.6 dynamic_slice.19
  129.0 8.8 %conditional.3 = ((f32[512,2]{0,1:T(2,128)S(1)}, f32[512,2]{0,1:T(2,128)S(1)}, f32[512,2,64]{0,2,1:T(8,128)S(1)})) conditional(s32[]{:T(128)} %convert_element_type.174, (f32[512,2]{0,1:T(2,128)S(1)}, f32[512,2]{0,1:T(2,128)S(1)}, f32[512,2,64]{0,2,1:T(8,128)S(1)}) %tuple.51, (s32[]{:T(128)}, s32[]{:T(128)}, s32[]{:T(128)}, ...), branch_computations={%region_1.1_spmd, %region_2.5_spmd} | conditional | flops 207981088 | bytes 14343918 | solution.py:116
  130.7 1.1 fusion.11
  131.8 1.2 fusion.14
  133.1 0.5 fusion.17
  133.6 0.6 fusion.33
  134.2 1.0 fusion.27
  135.1 0.6 fusion.34
  135.7 0.2 compare_and_fusion
  136.0 0.7 fusion.75
  136.7 0.4 fusion.5
  137.2 0.7 fusion.6
  137.8 0.6 dynamic_slice.19
  139.6 0.6 dynamic_slice.19
  141.4 0.6 dynamic_slice.19
  143.1 0.6 dynamic_slice.19
  144.9 0.6 dynamic_slice.19
  146.6 0.6 dynamic_slice.19
  148.4 0.6 dynamic_slice.19
  150.2 2.1 bitcast_convert_fusion
  152.2 0.0 reduce-scatter.3.cloned.1.call-update
  152.2 1.7 reduce-scatter.5.cloned.1.call-done
  153.9 59.0 %all-to-all-start.1 = ((bf16[8,68,512]{2,1,0:T(8,128)(2,1)}), bf16[8,68,512]{2,1,0:T(8,128)(2,1)S(1)}, u32[]{:S(2)}, u32[]{:S(2)}) async-start(bf16[8,68,512]{2,1,0:T(8,128)(2,1)} %reduce-scatter.5.cloned.1.call-done), calls=%async_computation.3 | async-start | bytes 1179648 | tf_op jit(solution)/shard_map/all_to_all | solution.py:167
  212.9 0.1 copy.23
  213.1 16.2 %all-to-all-done.1 = bf16[8,68,512]{2,1,0:T(8,128)(2,1)S(1)} async-done(((bf16[8,68,512]{2,1,0:T(8,128)(2,1)}), bf16[8,68,512]{2,1,0:T(8,128)(2,1)S(1)}, u32[]{:S(2)}, u32[]{:S(2)}) %all-to-all-start.1) | async-done | bytes 557088 | tf_op jit(solution)/shard_map/all_to_all | solution.py:167
  229.3 0.1 reshape.222
  229.4 2.0 gather_fusion.1
  231.4 0.7 reshape.223
  232.1 2.1 multiply_reduce_fusion
  234.1 6.1 %reduce-scatter.3.cloned.1.call-done = bf16[128,2048]{1,0:T(8,128)(2,1)} async-done(((bf16[512,2048]{1,0:T(8,128)(2,1)}), bf16[128,2048]{1,0:T(8,128)(2,1)}) %reduce-scatter.3.cloned.1.call-update) | async-done | bytes 524304 | tf_op jit(solution)/shard_map/reduce_scatter | solution.py:123
  (56 shorter events, 0.4 us)
Async XLA Ops:
  7.2 143.0 %copy-start = (bf16[2,64,2048]{2,1,0:T(8,128)(2,1)S(1)}, bf16[2,64,2048]{2,1,0:T(8,128)(2,1)}, u32[]{:S(2)}) copy-start(bf16[2,64,2048]{2,1,0:T(8,128)(2,1)} %param.22) | copy-start | bytes 1572868
  7.2 6.2 %copy-start.1 = (bf16[256,512]{1,0:T(8,128)(2,1)S(1)}, bf16[256,512]{1,0:T(8,128)(2,1)}, u32[]{:S(2)}) copy-start(bf16[256,512]{1,0:T(8,128)(2,1)} %param.23) | copy-start | bytes 786436
  7.2 55.7 %all-gather.5.cloned.1.call-start = ((), (), s32[]{:S(2)}) async-start(), calls=%async_computation.6 | async-start | bytes 2949120 | tf_op jit(solution)/shard_map/all_gather | solution.py:153
  16.5 48.8 %copy-start.8 = (f32[2048]{0:T(1024)S(1)}, f32[2048]{0:T(1024)}, u32[]{:S(2)}) copy-start(f32[2048]{0:T(1024)} %param.24) | copy-start | bytes 24580
  40.2 87.0 %all-gather.3.cloned.1.call-start = ((), (), s32[]{:S(2)}) async-start(), calls=%async_computation.4 | async-start | bytes 1081344 | tf_op jit(solution)/shard_map/all_gather | solution.py:66
  41.0 112.9 %reduce-scatter.5.cloned.1.call-start = ((), (), s32[]{:S(2)}) async-start(), calls=%async_computation.7 | async-start | bytes 2949120 | tf_op jit(solution)/shard_map/reduce_scatter | solution.py:164
  62.9 2.4 copy-start.2
  81.8 0.9 copy-start.3
  81.8 0.9 copy-start.4
  81.8 1.4 copy-start.6
  81.8 45.5 %copy-start.5 = (f32[128]{0:T(128)S(1)}, f32[128]{0:T(128)}, u32[]{:S(2)}) copy-start(f32[128]{0:T(128)} %param.20) | copy-start | bytes 1540
  81.8 158.5 %reduce-scatter.3.cloned.1.call-start = ((), (), s32[]{:S(2)}) async-start(), calls=%async_computation.5 | async-start | bytes 2621440 | tf_op jit(solution)/shard_map/reduce_scatter | solution.py:123
  152.2 60.7 %copy-start.7 = (f32[256,2]{0,1:T(2,128)S(1)}, f32[256,2]{0,1:T(2,128)}, u32[]{:S(2)}) copy-start(f32[256,2]{0,1:T(2,128)} %param.26) | copy-start | bytes 6148
  153.9 75.4 %all-to-all-start.1 = ((bf16[8,68,512]{2,1,0:T(8,128)(2,1)}), bf16[8,68,512]{2,1,0:T(8,128)(2,1)S(1)}, u32[]{:S(2)}, u32[]{:S(2)}) async-start(bf16[8,68,512]{2,1,0:T(8,128)(2,1)} %reduce-scatter.5.cloned.1.call-done), calls=%async_computation.3 | async-start | bytes 1179648 | tf_op jit(solution)/shard_map/all_to_all | solution.py:167
Sparse Core Ops, SparseCore 0:
  40.4 22.4 all-gather.4
  65.8 53.8 all-gather.2
  122.2 31.7 reduce-scatter.4
  156.9 83.3 reduce-scatter.2
where the time goes:
time: 248 us; the launch traced here: 247 us
  blocking collectives  67.8 us (27%)
  starting transfers between devices  59.1 us (24%)
  waiting for transfers between devices  46.7 us (19%)
  matrix products  21.6 us (9%)
  local copies, waits for them, and re-layouts  15.6 us (6%)
  between operations  14.1 us (6%)
  loops' own time  11.2 us (5%)
  other arithmetic  10.8 us (4%)
    all_to_all x1, starting transfers between devices, shards(): lax.all_to_all(summed, 'ep', split_axis=0, concat_axis=0, tiled=True)  59 us
    all_gather x1, blocking collectives, shards(): rope_piece = lax.all_gather(rope_key, ('ep', 'tp'), axis=0, tiled=True)  44.1 us
    all_to_all x1, blocking collectives, shards(): lax.all_to_all(send_rows, 'ep', split_axis=0, concat_axis=0, tiled=True)  23.7 us
    all_gather x1, waiting for transfers between devices, shards(): lax.all_gather(arrived, 'tp', axis=2, tiled=True).astype(jnp.float32)  21.8 us
    all_to_all x1, waiting for transfers between devices, shards(): lax.all_to_all(summed, 'ep', split_axis=0, concat_axis=0, tiled=True)  16.2 us
    dot_general x1, matrix products, shards(): jnp.einsum('scf,fd->scd', hidden, down_w[0], preferred_element_type=jnp.f...  10.5 us
    another operation x1, loops' own time, shards(): lax.scan(sub_block, initial, jnp.arange(0, piece_rows, sub_rows, dtype=jn...  9.28 us
    reduce_scatter x1, waiting for transfers between devices, shards(): lax.psum_scatter(jnp.einsum('thv,hvd->td', attn, mix_out, preferred_eleme...  6.14 us
  transfers between devices with their start and end apart: 5, of which 4 were waited for; matrix products, arithmetic and copies ran while one was open for 15% of the time, Pallas kernels for 0%

commit v1 on v0

v1 whole, which is shorter than its diff:
```python
import functools
import math

import jax
import jax.numpy as jnp
from jax import lax
from jax.experimental import pallas as pl
from jax.experimental.pallas import tpu as pltpu
from jax.sharding import PartitionSpec as P

D = 2048
NOPE = 64
SEQS = 1


eps = 1e-06
rope_base = 10000.0
neg_big = -1e30


def rotate(values, positions):
    half_dim = values.shape[-1] // 2
    inv_freq = rope_base ** (-jnp.arange(half_dim, dtype=jnp.float32) * 2.0 / values.shape[-1])
    angles = positions.astype(jnp.float32)[:, None] * inv_freq[None, :]
    angles = angles.reshape((angles.shape[0],) + (1,) * (values.ndim - 2) + (half_dim,))
    cosine = jnp.cos(angles)
    sine_part = jnp.sin(angles)
    first_half = values[..., :half_dim].astype(jnp.float32)
    second_half = values[..., half_dim:].astype(jnp.float32)
    return jnp.concatenate(
        [
            first_half * cosine - second_half * sine_part,
            second_half * cosine + first_half * sine_part,
        ],
        axis=-1,
    )


MESH = pl.DeviceIdType.MESH
VMEM = pltpu.VMEM


def greet(n_ep, n_tp):
    me = lax.axis_index("ep")
    t = lax.axis_index("tp")
    low, high = lax.rem(t, 2), lax.div(t, 2)
    n_high = n_tp // 2
    barrier = pltpu.get_barrier_semaphore()
    for k in range(1, n_ep):
        pl.semaphore_signal(
            barrier, inc=1, device_id={"ep": lax.rem(me + k, n_ep)}, device_id_type=MESH
        )
    for j in range(1, n_high):
        pl.semaphore_signal(
            barrier,
            inc=1,
            device_id={"tp": lax.rem(high + j, n_high) * 2 + low},
            device_id_type=MESH,
        )
    pl.semaphore_signal(barrier, inc=1, device_id={"tp": high * 2 + 1 - low}, device_id_type=MESH)
    pl.semaphore_wait(barrier, n_ep - 1 + n_high - 1 + 1)
    return me, t, low, high, n_high


def exchange_kernel(n_ep, n_tp, *refs):
    send_ref, kv_ref, out_ref, kvo_ref = refs[:4]
    own_sem, s1, r1, s2, r2, s3, r3 = refs[4:]
    me, t, low, high, n_high = greet(n_ep, n_tp)
    width = send_ref.shape[-1]

    def spot(kind, source, part):
        if kind == 0:
            start = pl.multiple_of(part * width, width)
            return out_ref.at[source, :, pl.ds(start, width)]
        return kvo_ref.at[source, part]

    def remote(src, dst, ssem, rsem, device):
        return pltpu.make_async_remote_copy(
            src_ref=src, dst_ref=dst, send_sem=ssem, recv_sem=rsem,
            device_id=device, device_id_type=MESH,
        )

    pending = []
    first = {}
    for kind in range(2):
        for k in range(1, n_ep):
            to = lax.rem(me + k, n_ep)
            src = send_ref.at[to] if kind == 0 else kv_ref
            copy = remote(src, spot(kind, me, t), s1.at[kind, k], r1.at[kind, k], {"ep": to})
            copy.start()
            first[kind, k] = copy
            pending.append(copy)
    local = []
    for kind in range(2):
        src = send_ref.at[me] if kind == 0 else kv_ref
        copy = pltpu.make_async_copy(src, spot(kind, me, t), own_sem.at[kind])
        copy.start()
        local.append(copy)
    partner = {"tp": high * 2 + 1 - low}
    second = {}

    def pass_on(kind, k):
        source = lax.rem(me - k + n_ep, n_ep)
        for j in range(1, n_high):
            from_high = lax.rem(high - j + n_high, n_high)
            second[kind, k, j].wait_recv()
            place = spot(kind, source, from_high * 2 + low)
            copy = remote(place, place, s3.at[kind, k, j], r3.at[kind, k, j], partner)
            copy.start()
            pending.append(copy)
            last.append(copy)

    last = []
    steps = [(kind, k) for kind in range(2) for k in range(n_ep)]
    for index, (kind, k) in enumerate(steps):
        source = lax.rem(me - k + n_ep, n_ep)
        if k == 0:
            local[kind].wait()
        else:
            first[kind, k].wait_recv()
        place = spot(kind, source, t)
        for j in range(1, n_high):
            to_high = lax.rem(high + j, n_high)
            copy = remote(
                place, place, s2.at[kind, k, j], r2.at[kind, k, j], {"tp": to_high * 2 + low}
            )
            copy.start()
            second[kind, k, j] = copy
            pending.append(copy)
        copy = remote(place, place, s3.at[kind, k, 0], r3.at[kind, k, 0], partner)
        copy.start()
        pending.append(copy)
        last.append(copy)
        if index >= 2:
            pass_on(*steps[index - 2])
    for step in steps[-2:]:
        pass_on(*step)
    for copy in last:
        copy.wait_recv()
    for copy in pending:
        copy.wait_send()


def exchange(send_rows, kv_pack, n_ep, n_tp):
    slots, width = send_rows.shape[1:]
    n_high = n_tp // 2
    sem = pltpu.SemaphoreType.DMA
    return pl.pallas_call(
        functools.partial(exchange_kernel, n_ep, n_tp),
        out_shape=(
            jax.ShapeDtypeStruct((n_ep, slots, n_tp * width), send_rows.dtype),
            jax.ShapeDtypeStruct((n_ep, n_tp) + kv_pack.shape, kv_pack.dtype),
        ),
        in_specs=[pl.BlockSpec(memory_space=VMEM)] * 2,
        out_specs=(pl.BlockSpec(memory_space=VMEM),) * 2,
        scratch_shapes=[
            sem((2,)),
            sem((2, n_ep)), sem((2, n_ep)),
            sem((2, n_ep, n_high)), sem((2, n_ep, n_high)),
            sem((2, n_ep, n_high)), sem((2, n_ep, n_high)),
        ],
        compiler_params=pltpu.CompilerParams(collective_id=0, has_side_effects=True),
        name="exchange",
    )(send_rows, kv_pack)


def give_back_kernel(n_ep, n_tp, *refs):
    part_ref, mix_ref, ret_ref, mixed_ref = refs[:4]
    low_in, high_out, high_in, final, mlow_in, mhigh_out, mhigh_in = refs[4:11]
    sa, ra, sb, rb, sc, rc, own_sem = refs[11:]
    me, t, low, high, n_high = greet(n_ep, n_tp)
    width = ret_ref.shape[-1]
    rows = mixed_ref.shape[0]
    f32 = jnp.float32
    partner = {"tp": high * 2 + 1 - low}

    def remote(src, dst, ssem, rsem, device):
        return pltpu.make_async_remote_copy(
            src_ref=src, dst_ref=dst, send_sem=ssem, recv_sem=rsem,
            device_id=device, device_id_type=MESH,
        )

    def target(k):
        return lax.rem(me + k, n_ep)

    def piece(k, which):
        if k == n_ep:
            return mix_ref.at[pl.ds(pl.multiple_of(which * rows, rows), rows), :]
        start = pl.multiple_of(which * width, width)
        return part_ref.at[target(k), :, pl.ds(start, width)]

    pending = []
    order = [k for k in range(1, n_ep)] + [0, n_ep]
    stage_a, stage_b, stage_c = {}, {}, []
    for k in order:
        for j in range(n_high):
            which = lax.rem(high + j, n_high) * 2 + 1 - low
            dst = low_in.at[k, j] if k < n_ep else mlow_in.at[j]
            copy = remote(piece(k, which), dst, sa.at[k, j], ra.at[k, j], partner)
            copy.start()
            stage_a[k, j] = copy
            pending.append(copy)

    def to_high(k):
        for j in range(1, n_high):
            peer = lax.rem(high + j, n_high)
            stage_a[k, j].wait_recv()
            got = low_in.at[k, j] if k < n_ep else mlow_in.at[j]
            out = high_out.at[k, j] if k < n_ep else mhigh_out.at[j]
            mine = piece(k, peer * 2 + low)
            out[...] = (mine[...].astype(f32) + got[...].astype(f32)).astype(out.dtype)
            dst = high_in.at[k, j] if k < n_ep else mhigh_in.at[j]
            copy = remote(out, dst, sb.at[k, j], rb.at[k, j], {"tp": peer * 2 + low})
            copy.start()
            stage_b[k, j] = copy
            pending.append(copy)

    def finish(k):
        stage_a[k, 0].wait_recv()
        got = low_in.at[k, 0] if k < n_ep else mlow_in.at[0]
        total = piece(k, t)[...].astype(f32) + got[...].astype(f32)
        for j in range(1, n_high):
            stage_b[k, j].wait_recv()
            arrived = high_in.at[k, j] if k < n_ep else mhigh_in.at[j]
            total = total + arrived[...].astype(f32)
        if k == n_ep:
            mixed_ref[...] = total.astype(mixed_ref.dtype)
            return
        if k == 0:
            ret_ref[me] = total.astype(ret_ref.dtype)
            return
        final[k] = total.astype(final.dtype)
        copy = remote(final.at[k], ret_ref.at[me], sc.at[k], rc.at[k], {"ep": target(k)})
        copy.start()
        stage_c.append(copy)
        pending.append(copy)

    for k in order:
        to_high(k)
    for k in order:
        finish(k)
    for copy in stage_c:
        copy.wait_recv()
    for copy in pending:
        copy.wait_send()


def give_back(partial, mix_part, n_ep, n_tp):
    slots, wide = partial.shape[1:]
    width, rows = wide // n_tp, mix_part.shape[0] // n_tp
    n_high = n_tp // 2
    sem = pltpu.SemaphoreType.DMA
    kind = partial.dtype
    return pl.pallas_call(
        functools.partial(give_back_kernel, n_ep, n_tp),
        out_shape=(
            jax.ShapeDtypeStruct((n_ep, slots, width), kind),
            jax.ShapeDtypeStruct((rows, mix_part.shape[1]), kind),
        ),
        in_specs=[pl.BlockSpec(memory_space=VMEM)] * 2,
        out_specs=(pl.BlockSpec(memory_space=VMEM),) * 2,
        scratch_shapes=[
            VMEM((n_ep, n_high, slots, width), kind),
            VMEM((n_ep, n_high, slots, width), kind),
            VMEM((n_ep, n_high, slots, width), kind),
            VMEM((n_ep, slots, width), kind),
            VMEM((n_high, rows, mix_part.shape[1]), kind),
            VMEM((n_high, rows, mix_part.shape[1]), kind),
            VMEM((n_high, rows, mix_part.shape[1]), kind),
            sem((n_ep + 1, n_high)), sem((n_ep + 1, n_high)),
            sem((n_ep + 1, n_high)), sem((n_ep + 1, n_high)),
            sem((n_ep,)), sem((n_ep,)), sem((1,)),
        ],
        compiler_params=pltpu.CompilerParams(collective_id=1, has_side_effects=True),
        name="give_back",
    )(partial, mix_part)


def attend_kernel(scale, heads, nope, bounds_ref, q_ref, kv_ref, wk_ref, wv_ref, place_ref, mix_ref, out_ref):
    lat = wk_ref.shape[0]
    n_tp = kv_ref.shape[1]
    queries = q_ref.shape[-1]
    block = queries
    own = block // n_tp
    vdim = wv_ref.shape[0] // heads
    f32, bf16 = jnp.float32, jnp.bfloat16
    factor = scale * math.log2(math.e)

    def step(index, state, masked):
        latents = kv_ref[index, :, :own, :].reshape(block, lat)
        rope_rows = jnp.concatenate(
            [kv_ref[index, part, own:, :] for part in range(n_tp)], axis=1
        )
        rot = lax.dot_general(
            rope_rows, place_ref[...], (((0,), (0,)), ((), ())), preferred_element_type=f32
        )
        values = lax.dot_general(
            wv_ref[...], latents, (((1,), (1,)), ((), ())), preferred_element_type=f32
        ).astype(bf16)
        result = []
        for h in range(heads):
            top, total, weighted = state[h]
            keys = (
                jnp.dot(latents, wk_ref[:, h * lat:(h + 1) * lat], preferred_element_type=f32) + rot
            ).astype(bf16)
            scores = jnp.dot(keys, q_ref[h], preferred_element_type=f32)
            if masked:
                key_id = lax.broadcasted_iota(jnp.int32, scores.shape, 0)
                query_id = lax.broadcasted_iota(jnp.int32, scores.shape, 1)
                scores = jnp.where(key_id <= query_id, scores, neg_big)
            new_top = jnp.maximum(top, jnp.max(scores, axis=0, keepdims=True))
            probs = jnp.exp2((scores - new_top) * factor)
            shrink = jnp.exp2((top - new_top) * factor)
            total = total * shrink + jnp.sum(probs, axis=0, keepdims=True)
            weighted = weighted * shrink + jnp.dot(
                values[h * vdim:(h + 1) * vdim], probs.astype(bf16), preferred_element_type=f32
            )
            result.append((new_top, total, weighted))
        return tuple(result)

    state = tuple(
        (
            jnp.full((1, queries), neg_big, f32),
            jnp.zeros((1, queries), f32),
            jnp.zeros((vdim, queries), f32),
        )
        for _ in range(heads)
    )
    state = lax.fori_loop(
        bounds_ref[0], bounds_ref[1], lambda i, run: step(i, run, False), state
    )
    state = step(bounds_ref[1], state, True)
    attn = jnp.concatenate([weighted / total for _, total, weighted in state], axis=0)
    attn = attn.T.astype(bf16)
    out_ref[...] = jnp.dot(attn, mix_ref[...], preferred_element_type=f32).astype(out_ref.dtype)


def attend(bounds, q_rows, kv_all, key_up, value_up, place, mix, scale, heads, nope):
    queries = q_rows.shape[-1]
    return pl.pallas_call(
        functools.partial(attend_kernel, scale, heads, nope),
        out_shape=jax.ShapeDtypeStruct((queries, mix.shape[1]), jnp.bfloat16),
        in_specs=[pl.BlockSpec(memory_space=pltpu.SMEM)] + [pl.BlockSpec(memory_space=VMEM)] * 6,
        out_specs=pl.BlockSpec(memory_space=VMEM),
        name="attend",
    )(bounds, q_rows, kv_all, key_up, value_up, place, mix)


def shards(
    queries,
    kv_latent,
    rope_key,
    kv_gain,
    kv_up,
    mix_out,
    moe_in,
    moe_gain,
    routes,
    route_weights,
    gate_w,
    up_w,
    down_w,
):
    n_ep, n_tp = lax.axis_size("ep"), lax.axis_size("tp")
    f32, bf16 = jnp.float32, jnp.bfloat16
    block_rows, heads_here, head_dim = queries.shape
    lat = kv_latent.shape[1]
    rope_dim = rope_key.shape[1]
    seq_len = block_rows * n_ep // SEQS
    ep_index = lax.axis_index("ep")
    query_start = ep_index * block_rows

    rows_here = routes.shape[0]
    top_count = routes.shape[1]
    experts = gate_w.shape[0] * n_ep
    mean_slots = top_count * rows_here // experts
    capacity = mean_slots + max(mean_slots // 16, 1)
    count = rows_here * top_count
    chosen = routes.T.reshape(-1)
    onehot = chosen[:, None] == jnp.arange(experts, dtype=jnp.int32)[None, :]
    entry = jnp.arange(count, dtype=jnp.int32)
    earlier = (entry[None, :] < entry[:, None]).astype(bf16)
    before = jnp.dot(earlier, onehot.astype(bf16), preferred_element_type=f32)
    slot_rank = jnp.sum(jnp.where(onehot, before, 0.0), axis=1).astype(jnp.int32)
    slot_dest = (chosen * capacity + slot_rank).reshape(top_count, rows_here)
    slot_ids = (
        jnp.arange(experts, dtype=jnp.int32)[:, None] * capacity
        + jnp.arange(capacity, dtype=jnp.int32)[None, :]
    )
    pick = slot_ids[:, :, None] == slot_dest[0][None, None, :]
    for choice in range(1, top_count):
        pick = pick | (slot_ids[:, :, None] == slot_dest[choice][None, None, :])
    send_rows = jnp.einsum(
        "scr,rd->scd", pick.astype(bf16), moe_in, preferred_element_type=f32
    ).astype(bf16)

    own_rows = kv_latent.shape[0]
    own_start = query_start + lax.axis_index("tp") * own_rows
    own_ids = own_start + jnp.arange(own_rows, dtype=jnp.int32)
    latent_rows = kv_latent.astype(f32)
    normed = (
        latent_rows
        * lax.rsqrt(jnp.mean(latent_rows * latent_rows, axis=-1, keepdims=True) + eps)
        * kv_gain
    ).astype(bf16)
    key_rot = rotate(rope_key, own_ids % seq_len).astype(bf16)
    kv_pack = jnp.concatenate([normed, key_rot.T], axis=0)

    arrived, kv_all = exchange(send_rows, kv_pack, n_ep, n_tp)

    query_index = query_start + jnp.arange(block_rows, dtype=jnp.int32)
    query_rot = rotate(queries[..., NOPE:], query_index % seq_len).astype(bf16)
    q_rows = jnp.concatenate([queries[..., :NOPE], query_rot], axis=-1).transpose(1, 2, 0)
    q_rows = jnp.pad(q_rows, ((0, 0), (0, lat - head_dim), (0, 0)))
    key_up = jnp.pad(kv_up[..., :NOPE], ((0, 0), (0, 0), (0, lat - NOPE))).reshape(lat, -1)
    value_up = kv_up[..., NOPE:].transpose(1, 2, 0).reshape(-1, lat)
    place = jnp.eye(rope_dim, lat, k=NOPE, dtype=bf16)
    bounds = jnp.stack([query_start // seq_len * seq_len // block_rows, ep_index]).astype(jnp.int32)
    mix_part = attend(
        bounds, q_rows, kv_all, key_up, value_up, place,
        mix_out.reshape(-1, mix_out.shape[-1]), 1.0 / math.sqrt(head_dim), heads_here, NOPE,
    )

    piece_f = arrived.astype(f32)
    scaled = (piece_f * moe_gain).astype(bf16)
    gate_acc = jnp.einsum("scd,df->scf", scaled, gate_w[0], preferred_element_type=f32)
    up_acc = jnp.einsum("scd,df->scf", scaled, up_w[0], preferred_element_type=f32)
    squares = jnp.sum(piece_f * piece_f, axis=-1)
    row_scale = lax.rsqrt(squares / D + eps)[..., None]
    hidden = (jax.nn.silu(gate_acc * row_scale) * (up_acc * row_scale)).astype(bf16)
    partial_value = jnp.einsum(
        "scf,fd->scd", hidden, down_w[0], preferred_element_type=f32
    ).astype(bf16)

    returned, mixed = give_back(partial_value, mix_part, n_ep, n_tp)
    moe_out = 0.0
    for choice in range(top_count):
        find = slot_dest[choice][:, None, None] == slot_ids[None]
        picked = jnp.einsum("rsc,scd->rd", find.astype(bf16), returned, preferred_element_type=f32)
        moe_out = moe_out + picked * route_weights[:, choice:choice + 1]
    return (mixed, moe_out.astype(bf16))


def solution(mesh):
    in_specs = (
        P("ep", "tp", None),
        P(("ep", "tp"), None),
        P(("ep", "tp"), None),
        P(),
        P(None, "tp", None),
        P("tp", None, None),
        P("ep", "tp"),
        P(),
        P("ep", None),
        P("ep", None),
        P("ep", None, "tp"),
        P("ep", None, "tp"),
        P("ep", "tp", None),
    )
    out_specs = (P(("ep", "tp"), None), P("ep", "tp"))
    return jax.shard_map(shards, mesh=mesh, in_specs=in_specs, out_specs=out_specs, check_vma=False)
```

time: 248 us -> 129 us (0.52)
  Pallas kernels: 0 us -> 95.9 us
  blocking collectives: 67.8 us -> 0 us
  starting transfers between devices: 59.1 us -> 0 us
  waiting for transfers between devices: 46.7 us -> 0 us
  between operations: 14.1 us -> 0.82 us
  local copies, waits for them, and re-layouts: 15.6 us -> 3.89 us
  loops' own time: 11.2 us -> 0 us
  other arithmetic: 10.8 us -> 5.48 us
    pallas_call x0 -> x3, Pallas kernels: none -> 95.9 us  [the longest x1 51.7 us: give_back(): pl.pallas_call(functools.partial(give_back_kernel, n_ep, n_tp), out_shape...]
    all_to_all x1 -> x0, starting transfers between devices: 59 us -> none  [shards(): lax.all_to_all(summed, 'ep', split_axis=0, concat_axis=0, tiled=True)]
    all_gather x1 -> x0, blocking collectives: 44.1 us -> none  [shards(): rope_piece = lax.all_gather(rope_key, ('ep', 'tp'), axis=0, tiled=True)]
    all_to_all x1 -> x0, blocking collectives: 23.7 us -> none  [shards(): lax.all_to_all(send_rows, 'ep', split_axis=0, concat_axis=0, tiled=True)]
    all_gather x2 -> x0, waiting for transfers between devices: 21.8 us -> none  [the longest x1 21.8 us: shards(): lax.all_gather(arrived, 'tp', axis=2, tiled=True).astype(jnp.float32)]
    all_to_all x1 -> x0, waiting for transfers between devices: 16.2 us -> none  [shards(): lax.all_to_all(summed, 'ep', split_axis=0, concat_axis=0, tiled=True)]
    another operation x9 -> x0, loops' own time: 11.2 us -> none  [the longest x1 9.28 us: shards(): lax.scan(sub_block, initial, jnp.arange(0, piece_rows, sub_rows, dtype=jn...]
    reduce_scatter x2 -> x0, waiting for transfers between devices: 7.85 us -> none  [the longest x1 6.14 us: shards(): lax.psum_scatter(jnp.einsum('thv,hvd->td', attn, mix_out, preferred_eleme...]
  transfers between devices with their start and end apart: 5 -> 0, of which waited for: 4 -> 0; matrix products, arithmetic and copies ran while one was open for 15% -> 0% of each run, Pallas kernels for 0% -> 0%
where the time goes in v1:
time: 129 us
  Pallas kernels  95.9 us (74%)
  matrix products  22.7 us (18%)
  other arithmetic  5.48 us (4%)
  local copies, waits for them, and re-layouts  3.89 us (3%)
    pallas_call x1, Pallas kernels, give_back(): pl.pallas_call(functools.partial(give_back_kernel, n_ep, n_tp), out_shape...  51.7 us
    pallas_call x1, Pallas kernels, exchange(): pl.pallas_call(functools.partial(exchange_kernel, n_ep, n_tp), out_shape=...  39.3 us
    dot_general x1, matrix products, shards(): jnp.einsum('scf,fd->scd', hidden, down_w[0], preferred_element_type=f32)  10.5 us
    dot_general x1, matrix products, shards(): jnp.einsum('scd,df->scf', scaled, up_w[0], preferred_element_type=f32)  6.81 us
    pallas_call x1, Pallas kernels, attend(): pl.pallas_call(functools.partial(attend_kernel, scale, heads, nope), out_...  4.99 us
    dot_general x2, matrix products, shards(): jnp.einsum('rsc,scd->rd', find.astype(bf16), returned, preferred_element_...  3.91 us

profile of v1, /device:TPU:0, one launch (start us, length us, event | category | flops | bytes accessed | tf_op | source)
XLA Modules:
  0.0 128.8 jit_solution(4793223474054094807)
XLA Ops:
  0.6 0.0 copy-start
  0.6 0.7 copy.16
  1.4 0.3 fusion.25
  1.7 0.1 iota_add_fusion
  1.7 0.0 copy-done
  1.7 1.2 convolution_convert_fusion.refs_0_
  3.0 0.8 fusion.54
  3.8 0.9 fusion.41
  4.7 0.8 fusion.43
  5.5 0.6 pad_maximum_fusion.refs_1_
  6.2 39.3 %exchange.1 = (bf16[8,68,2048]{2,1,0:T(8,128)(2,1)}, bf16[8,4,160,128]{3,2,1,0:T(8,128)(2,1)}) custom-call(bf16[8,68,512]{2,1,0:T(8,128)(2,1)} %convolution_convert_fusion.refs_0_, bf16[160,128]{1,0:T(8,128)(2,1)} %pad_maximum_fusion.refs_1_), custom_call_target="tpu_custom_call" | custom-call | tf_op jit(solution)/shard_map/exchange/pallas_call | solution.py:148
  45.4 0.0 copy-start.1
  45.4 6.8 %fusion.4 = f32[8,68,896]{2,1,0:T(8,128)} fusion(bf16[1,2048,896]{2,1,0:T(8,128)(2,1)} %param.24, bf16[8,68,2048]{2,1,0:T(8,128)(2,1)} %get-tuple-element.6, f32[2048]{0:T(1024)} %param.20), kind=kOutput, calls=%fused_computation.6 | convolution fusion | flops 1999831040 | bytes 7856128 | tf_op jit(solution)/shard_map/scd,df->scf/dot_general | solution.py:427
  52.3 0.0 copy-done.1
  52.3 0.0 copy-start.7
  52.3 0.6 fusion.1
  52.8 0.1 copy-done.7
  53.0 0.0 copy-start.2
  53.0 0.0 slice-start
  53.0 0.0 copy-start.4
  53.0 0.0 copy-start.6
  53.0 10.5 %fusion.8.refs_0_ = bf16[8,68,2048]{2,1,0:T(8,128)(2,1)} fusion(bf16[1,896,2048]{2,1,0:T(8,128)(2,1)} %param.25, f32[8,68,896]{2,1,0:T(8,128)} %fusion.4, bf16[1,2048,896]{2,1,0:T(8,128)(2,1)} %param.23, bf16[8,68,2048]{2,1,0:T(8,128)(2,1)S(1)} %copy-done.1, f32[2048]{0:T(1024)S(1)} %copy-done.7, f32[8,68]{1,0:T(8,128)S(1)} %add_rsqrt_fusion), kind=kOutput, calls=%fused_computation.10 | convolution fusion | flops 4001333248 | bytes 13756544 | tf_op jit(solution)/shard_map/scf,fd->scd/dot_general | solution.py:431
  63.4 0.7 pad_add_fusion.bounds_ref
  64.1 0.2 multiply_cosine_fusion
  64.3 0.0 copy-done.2
  64.4 0.0 slice-done
  64.4 0.7 pad.8.q_ref
  65.1 0.0 copy-done.4
  65.1 0.0 copy-done.6
  65.1 0.1 broadcast_select_fusion
  65.2 0.6 copy.19
  65.8 0.1 slice_bitcast_fusion
  66.0 0.7 copy.15
  66.7 0.7 fusion.48.place_ref
  67.3 5.0 %attend.1.refs_1_ = bf16[512,2048]{1,0:T(8,128)(2,1)} custom-call(s32[2]{0:T(128)} %pad_add_fusion.bounds_ref, bf16[2,128,512]{2,1,0:T(8,128)(2,1)} %pad.8.q_ref, bf16[8,4,160,128]{3,2,1,0:T(8,128)(2,1)} %get-tuple-element.7.kv_ref, bf16[128,256]{1,0:T(8,128)(2,1)} %bitcast.55, bf16[128,128]{1,0:T(8,128)(2,1)} %bitcast.57, ...), custom_call_target="tpu_custom_call" | custom-call | tf_op jit(solution)/shard_map/attend/pallas_call | solution.py:340
  72.3 0.0 copy-start.5
  72.3 51.7 %give_back.1 = (bf16[8,68,512]{2,1,0:T(8,128)(2,1)}, bf16[128,2048]{1,0:T(8,128)(2,1)}) custom-call(bf16[8,68,2048]{2,1,0:T(8,128)(2,1)} %fusion.8.refs_0_, bf16[512,2048]{1,0:T(8,128)(2,1)} %attend.1.refs_1_), custom_call_target="tpu_custom_call" | custom-call | tf_op jit(solution)/shard_map/give_back/pallas_call | solution.py:254
  124.0 0.0 copy-start.3
  124.0 0.0 copy-done.5
  124.1 1.6 %fusion.23 = f32[256,512]{1,0:T(8,128)S(1)} fusion(bf16[8,68,512]{2,1,0:T(8,128)(2,1)} %get-tuple-element.9, s32[8,68]{1,0:T(8,128)S(1)} %iota_add_fusion, s32[256]{0:T(256)S(1)} %get-tuple-element.18, f32[256]{0:T(256)S(1)} %bitcast.62), kind=kOutput, calls=%fused_computation.17 | convolution fusion | flops 142876672 | bytes 1085568 | tf_op jit(solution)/shard_map/rsc,scd->rd/dot_general | solution.py:439
  125.7 2.3 %fusion.24 = bf16[256,512]{1,0:T(8,128)(2,1)} fusion(f32[256,512]{1,0:T(8,128)S(1)} %fusion.23, bf16[8,68,512]{2,1,0:T(8,128)(2,1)} %get-tuple-element.9, s32[256]{0:T(256)S(1)} %get-tuple-element.19, s32[8,68]{1,0:T(8,128)S(1)} %iota_add_fusion, f32[256]{0:T(256)S(1)} %bitcast.61), kind=kOutput, calls=%fused_computation.18 | convolution fusion | flops 143138816 | bytes 1347712 | tf_op jit(solution)/shard_map/rsc,scd->rd/dot_general | solution.py:439
  128.0 0.0 copy-done.3
  128.0 0.8 copy.21
  (13 shorter events, 0.1 us)
Async XLA Ops:
  0.6 1.1 copy-start
  45.4 6.8 %copy-start.1 = (bf16[8,68,2048]{2,1,0:T(8,128)(2,1)S(1)}, bf16[8,68,2048]{2,1,0:T(8,128)(2,1)}, u32[]{:S(2)}) copy-start(bf16[8,68,2048]{2,1,0:T(8,128)(2,1)} %get-tuple-element.6) | copy-start | bytes 6684676
  52.3 0.7 copy-start.7
  53.0 11.4 %copy-start.2 = (bf16[512,2,96]{0,2,1:T(8,128)(2,1)S(1)}, bf16[512,2,96]{0,2,1:T(8,128)(2,1)}, u32[]{:S(2)}) copy-start(bf16[512,2,96]{0,2,1:T(8,128)(2,1)} %param.13) | copy-start | bytes 589828
  53.0 11.4 %slice-start = ((bf16[512,2,96]{0,2,1:T(8,128)(2,1)}), bf16[512,2,64]{0,2,1:T(8,128)(2,1)S(1)}, s32[]{:S(2)}) async-start(bf16[512,2,96]{0,2,1:T(8,128)(2,1)} %param.13), calls=%async_computation | async-start | bytes 262144 | tf_op jit(solution)/shard_map/slice | solution.py:413
  53.0 12.2 %copy-start.4 = (bf16[128,2,128]{2,1,0:T(2,128)(2,1)S(1)}, bf16[128,2,128]{2,1,0:T(2,128)(2,1)}, u32[]{:S(2)}) copy-start(bf16[128,2,128]{2,1,0:T(2,128)(2,1)} %param.17) | copy-start | bytes 196612
  53.0 12.2 %copy-start.6 = (pred[128]{0:T(512)(128)(4,1)S(1)}, pred[128]{0:T(512)(128)(4,1)}, u32[]{:S(2)}) copy-start(pred[128]{0:T(512)(128)(4,1)} %constant.88.clone.1) | copy-start | bytes 388
  72.3 51.7 %copy-start.5 = (f32[256,2]{0,1:T(2,128)S(1)}, f32[256,2]{0,1:T(2,128)}, u32[]{:S(2)}) copy-start(f32[256,2]{0,1:T(2,128)} %param.22) | copy-start | bytes 6148
  124.0 3.9 %copy-start.3 = (bf16[128,2048]{1,0:T(8,128)(2,1)S(1)}, bf16[128,2048]{1,0:T(8,128)(2,1)}, u32[]{:S(2)}) copy-start(bf16[128,2048]{1,0:T(8,128)(2,1)} %get-tuple-element.22) | copy-start | bytes 1572868
